TPU v7x, 512 devices: a whole 4x4x16 slice. The times are simulated.
512 devices in a mesh: fs: 16 (over y, x), tp: 32 (over z, core).
Axes of the slice: x: 4, y: 4, z: 16, core: 2. Of those that a mesh axis runs over, the one named last changes fastest.
Arguments:
- tokens: bfloat16 [4096, 2048], P('fs', 'tp'), may hold values from -60 to 60
- norm_gain: float32 [2048], P('fs'), may hold values from 0.1 to 1.9
- gate_weight: float32 [16, 2048, 4096], P(None, 'fs', 'tp'), may hold values from -0.125 to 0.125
- up_weight: float32 [16, 2048, 4096], P(None, 'fs', 'tp'), may hold values from -0.125 to 0.125
- down_weight: float32 [16, 2048, 4096], P(None, 'fs', 'tp'), may hold values from -0.1875 to 0.1875
- route: int32 [4096, 2], P('fs'), may hold values from 0 to 15, all different within a row; in each aligned block of 256 rows (0 to 255, 256 to 511, ...) at most 64 rows name the same one
- route_weight: float32 [4096, 2], P('fs'), may hold values from 0.2 to 1
Outputs:
- mixed: bfloat16 [4096, 2048], P('fs', 'tp')
- gate_new: bfloat16 [16, 2048, 4096], P('fs', None, 'tp')
- up_new: bfloat16 [16, 2048, 4096], P('fs', None, 'tp')
- down_new: bfloat16 [16, 2048, 4096], P('fs', None, 'tp')
Inputs may be any that keep to these rules, and one draw needn't show every extreme that they name: `route`: the 2 experts of a row differ. In each aligned block of 256 rows (the tokens of one index of fs) no expert is named by more than 64 rows, a bound that some block reaches.
All inputs are finite; a program needn't handle non-finite values.
Results may differ from a plain program's by a relative error of at most 0.024.
Values may be sent and summed in bfloat16 or wider, within the bound.
A program may use at most 64 MiB of HBM per device.

v0:
```python
import jax
import jax.numpy as jnp
from jax import lax
from jax.sharding import Mesh
from jax.sharding import PartitionSpec as P

TP = ("tp_0", "tp_1")
epsilon = 1e-05


def sent_together(arrays, axis, split_dim, concat_dim, along):
    both = jnp.concatenate(arrays, axis=along)
    whole, at, done = (
        lax.all_to_all(both, axis, split_axis=split_dim, concat_axis=concat_dim, tiled=True),
        0,
        [],
    )
    for a in arrays:
        done.append(lax.slice_in_dim(whole, at, at + a.shape[along], axis=along))
        at += a.shape[along]
    return tuple(done)


def sent_to_all(x, axis):
    peers = lax.axis_size(axis)
    return lax.all_to_all(jnp.broadcast_to(x[None], (peers, *x.shape)), axis, 0, 0, tiled=True)


def taken_together(x, axis):
    return sent_to_all(x, axis).sum(axis=0)


def reduced_to_own(pieces, axes, turns):
    shape = [lax.axis_size(a) for a in axes]
    pieces = pieces.reshape(*shape, *pieces.shape[1:])
    pieces = pieces.transpose(*turns, *range(len(axes), pieces.ndim))
    pieces = pieces.reshape(-1, *pieces.shape[len(axes) :])
    for k in turns:
        pieces = lax.psum_scatter(pieces, axes[k], scatter_dimension=0, tiled=True)
    return pieces[0]


def in_blocks(x, dim, peers):
    shape = x.shape
    pieces = x.reshape(*shape[:dim], peers, shape[dim] // peers, *shape[dim + 1 :])
    return jnp.moveaxis(pieces, dim, 0)


def scatter_axes(x, axes, turns, dim):
    peers = lax.axis_size(axes)
    return reduced_to_own(in_blocks(x, dim, peers), axes, turns)


def slot_table(route, block_rows, expert_count):
    pair_ids = route.reshape(-1, block_rows * route.shape[1])
    onehot = (
        pair_ids[:, :, None] == jnp.arange(expert_count, dtype=jnp.int32)[None, None, :]
    ).astype(jnp.int32)
    before = jnp.cumsum(onehot, axis=1) - onehot
    return jnp.sum(before * onehot, axis=2).reshape(route.shape)


def body(tokens, norm_gain, gate_weight, up_weight, down_weight, route, route_weight):
    experts = gate_weight.shape[0]
    tok_rows = tokens.shape[0]
    columns = tokens.shape[1]
    fs_count = lax.axis_size("fs")
    capacity = 4 * tok_rows // fs_count
    gain_col = norm_gain[None, :, None]
    gate_cast = (gate_weight * gain_col).astype(jnp.bfloat16)
    up_cast = (up_weight * gain_col).astype(jnp.bfloat16)
    down_cast = down_weight.astype(jnp.bfloat16)
    gate_new, up_new, down_new = sent_together((gate_cast, up_cast, down_cast), "fs", 0, 1, 2)
    slot_of = slot_table(route, tok_rows, experts)
    target = route * capacity + slot_of
    slot_lanes = jnp.arange(experts * capacity, dtype=jnp.int32)
    slot_hits = target[:, :, None] == slot_lanes[None, None, :]
    token_iota = jnp.arange(tok_rows, dtype=jnp.int32)[:, None, None]
    lane_token = jnp.sum(jnp.where(slot_hits, token_iota + 1, 0), axis=(0, 1)) - 1
    lane_token = jnp.where(lane_token < 0, tok_rows, lane_token)
    combine = jnp.sum(jnp.where(slot_hits, route_weight[:, :, None], 0.0), axis=1)
    tok_float = tokens.astype(jnp.float32)
    square_sum = taken_together(jnp.sum(tok_float * tok_float, axis=1), TP)
    full_width = columns * lax.axis_size(TP)
    normed = (tok_float * lax.rsqrt(square_sum / full_width + epsilon)[:, None]).astype(
        jnp.bfloat16
    )
    padded = jnp.concatenate([normed, jnp.zeros((1, columns), jnp.bfloat16)], axis=0)
    outgoing = padded[lane_token].reshape(experts, capacity, columns)
    arrived = lax.all_to_all(outgoing, "fs", split_axis=0, concat_axis=0, tiled=True).reshape(
        -1, columns
    )
    gate_local = gate_new[0]
    up_local = up_new[0]
    piece_rows = lax.all_gather(arrived, TP, axis=1, tiled=True)
    gate_acc = jnp.dot(piece_rows, gate_local, preferred_element_type=jnp.float32)
    up_acc = jnp.dot(piece_rows, up_local, preferred_element_type=jnp.float32)
    hidden = (jax.nn.silu(gate_acc) * up_acc).astype(jnp.bfloat16)
    down_local = down_new[0]
    summed = scatter_axes(
        lax.dot_general(
            down_local, hidden, (((1,), (1,)), ((), ())), preferred_element_type=jnp.float32
        ).astype(jnp.bfloat16),
        TP,
        (1, 0),
        0,
    ).astype(jnp.float32)
    own_columns = summed.shape[0]
    outgoing_back = summed.astype(jnp.bfloat16).reshape(own_columns, fs_count, capacity)
    returned = lax.all_to_all(outgoing_back, "fs", split_axis=1, concat_axis=1, tiled=True).reshape(
        own_columns, experts * capacity
    )
    mixed = lax.dot_general(
        combine,
        returned.astype(jnp.float32),
        (((1,), (1,)), ((), ())),
        preferred_element_type=jnp.float32,
    )
    return (mixed.astype(jnp.bfloat16), gate_new, up_new, down_new)


def solution(mesh):
    split = Mesh(mesh.devices.reshape(mesh.shape["fs"], 16, 2), ("fs", "tp_0", "tp_1"))
    in_specs = (
        P("fs", TP),
        P("fs"),
        P(None, "fs", TP),
        P(None, "fs", TP),
        P(None, "fs", TP),
        P("fs", None),
        P("fs", None),
    )
    out_specs = (P("fs", TP), P("fs", None, TP), P("fs", None, TP), P("fs", None, TP))
    return jax.shard_map(body, mesh=split, in_specs=in_specs, out_specs=out_specs, check_vma=False)
```

profile of v0, /device:TPU:32, one launch (start us, length us, event | category | flops | bytes accessed | tf_op | source)
XLA Modules:
  0.0 259.3 jit_solution(12488290934281086768)
XLA Ops:
  7.2 0.8 fusion.12
  7.9 0.6 broadcast_in_dim.45
  8.6 15.4 %all-to-all-start.1 = ((f32[32,1,256]{2,1,0:T(1,128)}), f32[32,1,256]{2,1,0:T(1,128)S(1)}, u32[]{:S(2)}, u32[]{:S(2)}) async-start(f32[32,1,256]{2,1,0:T(1,128)} %broadcast_in_dim.45), calls=%async_computation.1 | async-start | bytes 65536 | tf_op jit(solution)/shard_map/all_to_all | solution.py:26
  23.9 0.0 all-gather.2.cloned.1.call-start
  24.0 0.8 copy.71
  24.8 0.1 eq.40
  25.0 1.2 reduce-window.6
  26.2 0.2 slice_reduce_fusion
  26.5 0.1 copy.74
  26.5 0.1 broadcast.115
  26.6 0.1 fusion.14
  26.7 0.1 reshape.194
  26.9 0.1 copy.75
  26.9 0.7 multiply_add_fusion
  27.6 0.3 select_reduce_fusion
  28.0 7.7 %all-to-all-done.1 = f32[32,1,256]{2,1,0:T(1,128)S(1)} async-done(((f32[32,1,256]{2,1,0:T(1,128)}), f32[32,1,256]{2,1,0:T(1,128)S(1)}, u32[]{:S(2)}, u32[]{:S(2)}) %all-to-all-start.1) | async-done | bytes 32800 | tf_op jit(solution)/shard_map/all_to_all | solution.py:26
  35.7 0.1 reduce_sum.48
  35.8 0.8 fusion.13
  36.5 0.1 copy.84
  36.7 3.2 %gather_fusion = bf16[1024,64]{1,0:T(8,128)(2,1)S(1)} fusion(bf16[257,64]{1,0:T(8,128)(2,1)S(1)} %concatenate.7.clone, s32[1024]{0:T(1024)S(1)} %broadcast_clamp_fusion), kind=kCustom, calls=%fused_computation | custom fusion | bytes 266240 | tf_op jit(solution)/shard_map/gather | solution.py:89
  39.9 0.2 reshape.209
  40.2 15.1 %all_to_all.28 = bf16[16,2,2048]{2,1,0:T(2,128)(2,1)} all-to-all(bf16[16,2,2048]{2,1,0:T(2,128)(2,1)S(1)} %reshape.209), channel_id=1, replica_groups=mesh['fs'=16,'tp_0'=16,'tp_1'=2] {'fs'}, dimensions={0} | all-to-all | bytes 262144 | tf_op jit(solution)/shard_map/all_to_all | solution.py:90
  55.2 1.1 reshape.210
  56.4 0.8 copy.82
  57.1 0.0 all-gather.2.cloned.1.call-update
  57.2 0.0 reduce-scatter.3.cloned.1.call-start
  57.2 0.1 convert_element_type.41
  57.3 0.3 multiply_convert_fusion.1
  57.7 0.2 pad_maximum_fusion
  57.9 24.3 %all_to_all.29 = bf16[16,128,384]{2,1,0:T(8,128)(2,1)S(1)} all-to-all(bf16[16,128,384]{2,1,0:T(8,128)(2,1)S(1)} %pad_maximum_fusion), channel_id=1, replica_groups=mesh['fs'=16,'tp_0'=16,'tp_1'=2] {'fs'}, dimensions={0} | all-to-all | bytes 3145728 | tf_op jit(solution)/shard_map/all_to_all | solution.py:14
  82.3 0.3 fusion.16
  82.6 37.4 %all-gather.2.cloned.1.call-done = bf16[1024,2048]{0,1:T(8,128)(2,1)} async-done(((bf16[1024,64]{0,1:T(8,128)(2,1)}), bf16[1024,2048]{0,1:T(8,128)(2,1)}) %all-gather.2.cloned.1.call-update) | async-done | bytes 4194320 | tf_op jit(solution)/shard_map/all_gather | solution.py:95
  120.0 3.5 %fusion.3 = f32[1024,128]{1,0:T(8,128)S(1)} fusion(bf16[1024,2048]{0,1:T(8,128)(2,1)} %all-gather.2.cloned.1.call-done, bf16[1,2048,128]{2,1,0:T(8,128)(2,1)S(1)} %get-tuple-element.4), kind=kOutput, calls=%fused_computation.12 | convolution fusion | flops 536870912 | bytes 5242880 | tf_op jit(solution)/shard_map/dot_general | solution.py:96
  123.5 8.6 %convolution_convert_fusion = bf16[2048,1024]{1,0:T(8,128)(2,1)} fusion(bf16[1024,2048]{0,1:T(8,128)(2,1)} %all-gather.2.cloned.1.call-done, bf16[1,2048,128]{2,1,0:T(8,128)(2,1)S(1)} %get-tuple-element.5, bf16[1,2048,128]{2,1,0:T(8,128)(2,1)S(1)} %get-tuple-element.6, f32[1024,128]{1,0:T(8,128)S(1)} %fusion.3), kind=kOutput, calls=%fused_computation.1 | convolution fusion | flops 1076625408 | bytes 9961472 | tf_op jit(solution)/shard_map/dot_general | solution.py:101
  132.1 4.8 %copy.79 = bf16[16,2,64,1024]{3,2,0,1:T(8,128)(2,1)} copy(bf16[16,2,64,1024]{3,2,1,0:T(8,128)(2,1)} %bitcast.42) | data formatting | bytes 8388608 | tf_op jit(solution)/shard_map/reshape;reshape | solution.py:35
  137.0 0.0 reduce-scatter.5.cloned.1.call-start
  137.0 19.7 %reduce-scatter.3.cloned.1.call-done = bf16[16,64,1024]{2,1,0:T(8,128)(2,1)} async-done(((bf16[32,64,1024]{2,1,0:T(8,128)(2,1)}), bf16[16,64,1024]{2,1,0:T(8,128)(2,1)}) %reduce-scatter.3.cloned.1.call-update) | async-done | bytes 2097168 | tf_op jit(solution)/shard_map/reduce_scatter | solution.py:39
  156.7 77.7 %reduce-scatter.5.cloned.1.call-done = bf16[1,64,1024]{2,1,0:T(8,128)(2,1)} async-done(((bf16[16,64,1024]{2,1,0:T(8,128)(2,1)}), bf16[1,64,1024]{2,1,0:T(8,128)(2,1)}) %reduce-scatter.5.cloned.1.call-update) | async-done | bytes 131088 | tf_op jit(solution)/shard_map/reduce_scatter | solution.py:39
  234.4 1.1 reshape.198
  235.5 0.1 copy.86
  235.6 0.9 reshape.211
  236.5 6.8 %all-to-all-start.3 = ((bf16[16,2,2048]{2,1,0:T(2,128)(2,1)}), bf16[16,2,2048]{2,1,0:T(2,128)(2,1)S(1)}, u32[]{:S(2)}, u32[]{:S(2)}) async-start(bf16[16,2,2048]{2,1,0:T(2,128)(2,1)} %reshape.211), calls=%async_computation.5 | async-start | bytes 262144 | tf_op jit(solution)/shard_map/all_to_all | solution.py:110
  243.3 0.3 select_reduce_fusion.1
  243.6 7.7 %all-to-all-done.3 = bf16[16,2,2048]{2,1,0:T(2,128)(2,1)S(1)} async-done(((bf16[16,2,2048]{2,1,0:T(2,128)(2,1)}), bf16[16,2,2048]{2,1,0:T(2,128)(2,1)S(1)}, u32[]{:S(2)}, u32[]{:S(2)}) %all-to-all-start.3) | async-done | bytes 131104 | tf_op jit(solution)/shard_map/all_to_all | solution.py:110
  251.3 0.2 reshape.212
  251.5 0.2 copy.81
  251.7 0.2 reshape.199
  251.9 0.9 fusion.17
  (29 shorter events, 0.2 us)
Async XLA Ops:
  8.6 27.1 %all-to-all-start.1 = ((f32[32,1,256]{2,1,0:T(1,128)}), f32[32,1,256]{2,1,0:T(1,128)S(1)}, u32[]{:S(2)}, u32[]{:S(2)}) async-start(f32[32,1,256]{2,1,0:T(1,128)} %broadcast_in_dim.45), calls=%async_computation.1 | async-start | bytes 65536 | tf_op jit(solution)/shard_map/all_to_all | solution.py:26
  23.9 96.1 %all-gather.2.cloned.1.call-start = ((), (), s32[]{:S(2)}) async-start(), calls=%async_computation.6 | async-start | bytes 4325376 | tf_op jit(solution)/shard_map/all_gather | solution.py:95
  36.5 20.7 %copy-start.3 = (f32[16,128,128]{2,1,0:T(8,128)S(1)}, f32[16,128,128]{2,1,0:T(8,128)}, u32[]{:S(2)}) copy-start(f32[16,128,128]{2,1,0:T(8,128)} %param.11) | copy-start | bytes 3145732
  39.9 17.4 %copy-start.4 = (f32[16,128,128]{2,1,0:T(8,128)S(1)}, f32[16,128,128]{2,1,0:T(8,128)}, u32[]{:S(2)}) copy-start(f32[16,128,128]{2,1,0:T(8,128)} %param.9) | copy-start | bytes 3145732
  39.9 17.4 %copy-start.5 = (f32[16,128,128]{2,1,0:T(8,128)S(1)}, f32[16,128,128]{2,1,0:T(8,128)}, u32[]{:S(2)}) copy-start(f32[16,128,128]{2,1,0:T(8,128)} %param.10) | copy-start | bytes 3145732
  39.9 17.4 %copy-start.7 = (f32[128]{0:T(128)S(1)}, f32[128]{0:T(128)}, u32[]{:S(2)}) copy-start(f32[128]{0:T(128)} %param.8) | copy-start | bytes 1540
  57.2 99.5 %reduce-scatter.3.cloned.1.call-start = ((), (), s32[]{:S(2)}) async-start(), calls=%async_computation.7 | async-start | bytes 6291456 | tf_op jit(solution)/shard_map/reduce_scatter | solution.py:39
  82.6 40.9 %copy-start = (bf16[1,2048,128]{2,1,0:T(8,128)(2,1)}, bf16[1,2048,128]{2,1,0:T(8,128)(2,1)S(1)}, u32[]{:S(2)}) copy-start(bf16[1,2048,128]{2,1,0:T(8,128)(2,1)S(1)} %get-tuple-element.4) | copy-start | bytes 1572868
  82.6 40.9 %copy-start.1 = (bf16[1,2048,128]{2,1,0:T(8,128)(2,1)}, bf16[1,2048,128]{2,1,0:T(8,128)(2,1)S(1)}, u32[]{:S(2)}) copy-start(bf16[1,2048,128]{2,1,0:T(8,128)(2,1)S(1)} %get-tuple-element.5) | copy-start | bytes 1572868
  82.6 40.9 %copy-start.2 = (bf16[1,2048,128]{2,1,0:T(8,128)(2,1)}, bf16[1,2048,128]{2,1,0:T(8,128)(2,1)S(1)}, u32[]{:S(2)}) copy-start(bf16[1,2048,128]{2,1,0:T(8,128)(2,1)S(1)} %get-tuple-element.6) | copy-start | bytes 1572868
  137.0 106.3 %copy-start.6 = (f32[256,2]{0,1:T(2,128)S(1)}, f32[256,2]{0,1:T(2,128)}, u32[]{:S(2)}) copy-start(f32[256,2]{0,1:T(2,128)} %param.13) | copy-start | bytes 6148
  137.0 97.4 %reduce-scatter.5.cloned.1.call-start = ((), (), s32[]{:S(2)}) async-start(), calls=%async_computation.8 | async-start | bytes 2228224 | tf_op jit(solution)/shard_map/reduce_scatter | solution.py:39
  236.5 14.8 %all-to-all-start.3 = ((bf16[16,2,2048]{2,1,0:T(2,128)(2,1)}), bf16[16,2,2048]{2,1,0:T(2,128)(2,1)S(1)}, u32[]{:S(2)}, u32[]{:S(2)}) async-start(bf16[16,2,2048]{2,1,0:T(2,128)(2,1)} %reshape.211), calls=%async_computation.5 | async-start | bytes 262144 | tf_op jit(solution)/shard_map/all_to_all | solution.py:110
Sparse Core Ops, SparseCore 0:
  57.3 62.7 all-gather.1
  137.1 19.5 reduce-scatter.2
  159.5 74.8 reduce-scatter.4
where the time goes:
time: 260 us; the launch traced here: 259 us
  waiting for transfers between devices  150 us (58%)
  blocking collectives  39.4 us (15%)
  starting transfers between devices  22.3 us (9%)
  local copies, waits for them, and re-layouts  15.5 us (6%)
  between operations  14.1 us (5%)
  matrix products  13 us (5%)
  other arithmetic  4.87 us (2%)
    reduce_scatter x2, waiting for transfers between devices, reduced_to_own(): pieces = lax.psum_scatter(pieces, axes[k], scatter_dimension=0, tiled=True)  97.4 us
    all_gather x1, waiting for transfers between devices, body(): piece_rows = lax.all_gather(arrived, TP, axis=1, tiled=True)  37.4 us
    all_to_all x1, blocking collectives, sent_together(): lax.all_to_all(both, axis, split_axis=split_dim, concat_axis=concat_dim,...  24.3 us
    all_to_all x1, starting transfers between devices, sent_to_all(): lax.all_to_all(jnp.broadcast_to(x[None], (peers, *x.shape)), axis, 0, 0,...  15.4 us
    all_to_all x1, blocking collectives, body(): lax.all_to_all(outgoing, 'fs', split_axis=0, concat_axis=0, tiled=True)  15.1 us
    dot_general x1, matrix products, body(): lax.dot_general(down_local, hidden, (((1,), (1,)), ((), ())), preferred_e...  8.59 us
    all_to_all x1, waiting for transfers between devices, sent_to_all(): lax.all_to_all(jnp.broadcast_to(x[None], (peers, *x.shape)), axis, 0, 0,...  7.74 us
    all_to_all x1, waiting for transfers between devices, body(): lax.all_to_all(outgoing_back, 'fs', split_axis=1, concat_axis=1, tiled=True)  7.69 us
  transfers between devices with their start and end apart: 5, of which 5 were waited for; matrix products, arithmetic and copies ran while one was open for 2% of the time, Pallas kernels for 0%

commit v1 on v0

--- a/solution.py
+++ b/solution.py
@@ -92,7 +92,9 @@
     )
     gate_local = gate_new[0]
     up_local = up_new[0]
-    piece_rows = lax.all_gather(arrived, TP, axis=1, tiled=True)
+    piece_rows = jnp.concatenate(
+        lax.all_to_all(jnp.stack([arrived] * lax.axis_size(TP)), TP, 0, 0), axis=1
+    )
     gate_acc = jnp.dot(piece_rows, gate_local, preferred_element_type=jnp.float32)
     up_acc = jnp.dot(piece_rows, up_local, preferred_element_type=jnp.float32)
     hidden = (jax.nn.silu(gate_acc) * up_acc).astype(jnp.bfloat16)

time: 260 us -> 413 us (1.59)
  the two profiles are of different devices: /device:TPU:32 before, /device:TPU:2 now
where the time goes in v1:
time: 413 us
  waiting for transfers between devices  318 us (77%)
  starting transfers between devices  42.1 us (10%)
  local copies, waits for them, and re-layouts  17.1 us (4%)
  between operations  14.3 us (3%)
  matrix products  13 us (3%)
  other arithmetic  7.81 us (2%)
    all_to_all x1, waiting for transfers between devices, body(): lax.all_to_all(jnp.stack([arrived] * lax.axis_size(TP)), TP, 0, 0)  183 us
    reduce_scatter x2, waiting for transfers between devices, reduced_to_own(): pieces = lax.psum_scatter(pieces, axes[k], scatter_dimension=0, tiled=True)  97.8 us
    all_to_all x1, waiting for transfers between devices, sent_together(): lax.all_to_all(both, axis, split_axis=split_dim, concat_axis=concat_dim,...  19.6 us
    all_to_all x1, starting transfers between devices, sent_to_all(): lax.all_to_all(jnp.broadcast_to(x[None], (peers, *x.shape)), axis, 0, 0,...  15.5 us
    dot_general x1, matrix products, body(): lax.dot_general(down_local, hidden, (((1,), (1,)), ((), ())), preferred_e...  8.59 us
  transfers between devices with their start and end apart: 7, of which 7 were waited for; matrix products, arithmetic and copies ran while one was open for 2% of the time, Pallas kernels for 0%

profile of v1, /device:TPU:2, one launch (start us, length us, event | category | flops | bytes accessed | tf_op | source)
XLA Modules:
  0.0 412.5 jit_solution(13219871085599472936)
XLA Ops:
  7.2 0.9 fusion.12
  8.1 0.6 broadcast_in_dim.45
  8.7 15.5 %all-to-all-start.1 = ((f32[32,1,256]{2,1,0:T(1,128)}), f32[32,1,256]{2,1,0:T(1,128)S(1)}, u32[]{:S(2)}, u32[]{:S(2)}) async-start(f32[32,1,256]{2,1,0:T(1,128)} %broadcast_in_dim.45), calls=%async_computation.1 | async-start | bytes 65536 | tf_op jit(solution)/shard_map/all_to_all | solution.py:26
  24.2 0.8 copy.72
  25.0 0.1 eq.40
  25.2 1.2 reduce-window.6
  26.3 0.2 slice_reduce_fusion
  26.6 0.1 copy.75
  26.7 0.1 broadcast.116
  26.8 0.1 fusion.14
  26.9 0.1 reshape.199
  27.0 0.1 copy.76
  27.1 0.7 multiply_add_fusion
  27.8 0.3 select_reduce_fusion
  28.1 1.3 convert_element_type.41
  29.5 1.6 multiply_convert_fusion.1
  31.1 6.1 %all-to-all-done.1 = f32[32,1,256]{2,1,0:T(1,128)S(1)} async-done(((f32[32,1,256]{2,1,0:T(1,128)}), f32[32,1,256]{2,1,0:T(1,128)S(1)}, u32[]{:S(2)}, u32[]{:S(2)}) %all-to-all-start.1) | async-done | bytes 32800 | tf_op jit(solution)/shard_map/all_to_all | solution.py:26
  37.2 0.1 reduce_sum.48
  37.2 0.1 copy.84
  37.4 3.2 gather_fusion
  40.6 0.9 reshape.215
  41.5 7.5 %all-to-all-start.2 = ((bf16[16,2,2048]{2,1,0:T(2,128)(2,1)}), bf16[16,2,2048]{2,1,0:T(2,128)(2,1)S(1)}, u32[]{:S(2)}, u32[]{:S(2)}) async-start(bf16[16,2,2048]{2,1,0:T(2,128)(2,1)} %reshape.215), calls=%async_computation.2 | async-start | bytes 262144 | tf_op jit(solution)/shard_map/all_to_all | solution.py:90
  49.0 1.4 pad_maximum_fusion
  50.4 5.2 %all-to-all-done.2 = bf16[16,2,2048]{2,1,0:T(2,128)(2,1)S(1)} async-done(((bf16[16,2,2048]{2,1,0:T(2,128)(2,1)}), bf16[16,2,2048]{2,1,0:T(2,128)(2,1)S(1)}, u32[]{:S(2)}, u32[]{:S(2)}) %all-to-all-start.2) | async-done | bytes 131104 | tf_op jit(solution)/shard_map/all_to_all | solution.py:90
  55.6 5.0 %all-to-all-start = ((bf16[16,128,384]{2,1,0:T(8,128)(2,1)}), bf16[16,128,384]{2,1,0:T(8,128)(2,1)S(1)}, u32[]{:S(2)}, u32[]{:S(2)}) async-start(bf16[16,128,384]{2,1,0:T(8,128)(2,1)} %pad_maximum_fusion), calls=%async_computation | async-start | bytes 3145728 | tf_op jit(solution)/shard_map/all_to_all | solution.py:14
  60.6 0.2 reshape.216
  60.8 0.1 copy.79
  60.9 19.6 %all-to-all-done = bf16[16,128,384]{2,1,0:T(8,128)(2,1)S(1)} async-done(((bf16[16,128,384]{2,1,0:T(8,128)(2,1)}), bf16[16,128,384]{2,1,0:T(8,128)(2,1)S(1)}, u32[]{:S(2)}, u32[]{:S(2)}) %all-to-all-start) | async-done | bytes 1572896 | tf_op jit(solution)/shard_map/all_to_all | solution.py:14
  80.5 2.5 stack.3
  83.0 7.0 %all-to-all-start.3 = ((bf16[32,1024,64]{1,2,0:T(8,128)(2,1)}), bf16[32,1024,64]{1,2,0:T(8,128)(2,1)}, u32[]{:S(2)}, u32[]{:S(2)}) async-start(bf16[32,1024,64]{1,2,0:T(8,128)(2,1)} %stack.3), calls=%async_computation.3 | async-start | bytes 8388608 | tf_op jit(solution)/shard_map/all_to_all | solution.py:96
  90.1 0.3 fusion.16
  90.4 183.1 %all-to-all-done.3 = bf16[32,1024,64]{1,2,0:T(8,128)(2,1)} async-done(((bf16[32,1024,64]{1,2,0:T(8,128)(2,1)}), bf16[32,1024,64]{1,2,0:T(8,128)(2,1)}, u32[]{:S(2)}, u32[]{:S(2)}) %all-to-all-start.3) | async-done | bytes 4194336 | tf_op jit(solution)/shard_map/all_to_all | solution.py:96
  273.5 3.5 fusion.3
  277.0 8.6 %convolution_convert_fusion = bf16[2048,1024]{1,0:T(8,128)(2,1)} fusion(bf16[1024,2048]{0,1:T(8,128)(2,1)} %bitcast.13, bf16[1,2048,128]{2,1,0:T(8,128)(2,1)S(1)} %get-tuple-element.5, bf16[1,2048,128]{2,1,0:T(8,128)(2,1)S(1)} %get-tuple-element.6, f32[1024,128]{1,0:T(8,128)S(1)} %fusion.3), kind=kOutput, calls=%fused_computation.1 | convolution fusion | flops 1076625408 | bytes 9961472 | tf_op jit(solution)/shard_map/dot_general | solution.py:103
  285.6 4.8 %copy.80 = bf16[16,2,64,1024]{3,2,0,1:T(8,128)(2,1)} copy(bf16[16,2,64,1024]{3,2,1,0:T(8,128)(2,1)} %bitcast.45) | data formatting | bytes 8388608 | tf_op jit(solution)/shard_map/reshape;reshape | solution.py:35
  290.4 0.0 reduce-scatter.5.cloned.1.call-start
  290.5 19.5 %reduce-scatter.3.cloned.1.call-done = bf16[16,64,1024]{2,1,0:T(8,128)(2,1)} async-done(((bf16[32,64,1024]{2,1,0:T(8,128)(2,1)}), bf16[16,64,1024]{2,1,0:T(8,128)(2,1)}) %reduce-scatter.3.cloned.1.call-update) | async-done | bytes 2097168 | tf_op jit(solution)/shard_map/reduce_scatter | solution.py:39
  310.0 78.4 %reduce-scatter.5.cloned.1.call-done = bf16[1,64,1024]{2,1,0:T(8,128)(2,1)} async-done(((bf16[16,64,1024]{2,1,0:T(8,128)(2,1)}), bf16[1,64,1024]{2,1,0:T(8,128)(2,1)}) %reduce-scatter.5.cloned.1.call-update) | async-done | bytes 131088 | tf_op jit(solution)/shard_map/reduce_scatter | solution.py:39
  388.3 1.1 reshape.204
  389.5 0.1 copy.86
  389.5 0.9 reshape.217
  390.4 7.1 %all-to-all-start.4 = ((bf16[16,2,2048]{2,1,0:T(2,128)(2,1)}), bf16[16,2,2048]{2,1,0:T(2,128)(2,1)S(1)}, u32[]{:S(2)}, u32[]{:S(2)}) async-start(bf16[16,2,2048]{2,1,0:T(2,128)(2,1)} %reshape.217), calls=%async_computation.6 | async-start | bytes 262144 | tf_op jit(solution)/shard_map/all_to_all | solution.py:112
  397.6 0.3 select_reduce_fusion.1
  397.8 6.3 %all-to-all-done.4 = bf16[16,2,2048]{2,1,0:T(2,128)(2,1)S(1)} async-done(((bf16[16,2,2048]{2,1,0:T(2,128)(2,1)}), bf16[16,2,2048]{2,1,0:T(2,128)(2,1)S(1)}, u32[]{:S(2)}, u32[]{:S(2)}) %all-to-all-start.4) | async-done | bytes 131104 | tf_op jit(solution)/shard_map/all_to_all | solution.py:112
  404.2 0.2 reshape.218
  404.4 0.2 copy.82
  404.6 0.2 reshape.205
  404.8 0.9 fusion.17
  (27 shorter events, 0.3 us)
Async XLA Ops:
  7.2 30.1 %copy-start.4 = (bf16[256,64]{0,1:T(8,128)(2,1)S(1)}, bf16[256,64]{0,1:T(8,128)(2,1)}, u32[]{:S(2)}) copy-start(bf16[256,64]{0,1:T(8,128)(2,1)} %param.7) | copy-start | bytes 98308
  7.2 22.3 %copy-start.3 = (f32[16,128,128]{2,1,0:T(8,128)S(1)}, f32[16,128,128]{2,1,0:T(8,128)}, u32[]{:S(2)}) copy-start(f32[16,128,128]{2,1,0:T(8,128)} %param.9) | copy-start | bytes 3145732
  8.7 28.5 %all-to-all-start.1 = ((f32[32,1,256]{2,1,0:T(1,128)}), f32[32,1,256]{2,1,0:T(1,128)S(1)}, u32[]{:S(2)}, u32[]{:S(2)}) async-start(f32[32,1,256]{2,1,0:T(1,128)} %broadcast_in_dim.45), calls=%async_computation.1 | async-start | bytes 65536 | tf_op jit(solution)/shard_map/all_to_all | solution.py:26
  41.5 14.1 %all-to-all-start.2 = ((bf16[16,2,2048]{2,1,0:T(2,128)(2,1)}), bf16[16,2,2048]{2,1,0:T(2,128)(2,1)S(1)}, u32[]{:S(2)}, u32[]{:S(2)}) async-start(bf16[16,2,2048]{2,1,0:T(2,128)(2,1)} %reshape.215), calls=%async_computation.2 | async-start | bytes 262144 | tf_op jit(solution)/shard_map/all_to_all | solution.py:90
  55.6 24.9 %all-to-all-start = ((bf16[16,128,384]{2,1,0:T(8,128)(2,1)}), bf16[16,128,384]{2,1,0:T(8,128)(2,1)S(1)}, u32[]{:S(2)}, u32[]{:S(2)}) async-start(bf16[16,128,384]{2,1,0:T(8,128)(2,1)} %pad_maximum_fusion), calls=%async_computation | async-start | bytes 3145728 | tf_op jit(solution)/shard_map/all_to_all | solution.py:14
  83.0 190.5 %all-to-all-start.3 = ((bf16[32,1024,64]{1,2,0:T(8,128)(2,1)}), bf16[32,1024,64]{1,2,0:T(8,128)(2,1)}, u32[]{:S(2)}, u32[]{:S(2)}) async-start(bf16[32,1024,64]{1,2,0:T(8,128)(2,1)} %stack.3), calls=%async_computation.3 | async-start | bytes 8388608 | tf_op jit(solution)/shard_map/all_to_all | solution.py:96
  90.0 219.9 %reduce-scatter.3.cloned.1.call-start = ((), (), s32[]{:S(2)}) async-start(), calls=%async_computation.7 | async-start | bytes 6291456 | tf_op jit(solution)/shard_map/reduce_scatter | solution.py:39
  90.4 195.2 %copy-start = (bf16[1,2048,128]{2,1,0:T(8,128)(2,1)}, bf16[1,2048,128]{2,1,0:T(8,128)(2,1)S(1)}, u32[]{:S(2)}) copy-start(bf16[1,2048,128]{2,1,0:T(8,128)(2,1)S(1)} %get-tuple-element.4) | copy-start | bytes 1572868
  90.4 195.2 %copy-start.1 = (bf16[1,2048,128]{2,1,0:T(8,128)(2,1)}, bf16[1,2048,128]{2,1,0:T(8,128)(2,1)S(1)}, u32[]{:S(2)}) copy-start(bf16[1,2048,128]{2,1,0:T(8,128)(2,1)S(1)} %get-tuple-element.5) | copy-start | bytes 1572868
  90.4 195.2 %copy-start.2 = (bf16[1,2048,128]{2,1,0:T(8,128)(2,1)}, bf16[1,2048,128]{2,1,0:T(8,128)(2,1)S(1)}, u32[]{:S(2)}) copy-start(bf16[1,2048,128]{2,1,0:T(8,128)(2,1)S(1)} %get-tuple-element.6) | copy-start | bytes 1572868
  290.4 107.1 %copy-start.5 = (f32[256,2]{0,1:T(2,128)S(1)}, f32[256,2]{0,1:T(2,128)}, u32[]{:S(2)}) copy-start(f32[256,2]{0,1:T(2,128)} %param.13) | copy-start | bytes 6148
  290.4 97.9 %reduce-scatter.5.cloned.1.call-start = ((), (), s32[]{:S(2)}) async-start(), calls=%async_computation.8 | async-start | bytes 2228224 | tf_op jit(solution)/shard_map/reduce_scatter | solution.py:39
  390.4 13.7 %all-to-all-start.4 = ((bf16[16,2,2048]{2,1,0:T(2,128)(2,1)}), bf16[16,2,2048]{2,1,0:T(2,128)(2,1)S(1)}, u32[]{:S(2)}, u32[]{:S(2)}) async-start(bf16[16,2,2048]{2,1,0:T(2,128)(2,1)} %reshape.217), calls=%async_computation.6 | async-start | bytes 262144 | tf_op jit(solution)/shard_map/all_to_all | solution.py:112
Sparse Core Ops, SparseCore 0:
  290.6 19.3 reduce-scatter.2
  312.8 75.5 reduce-scatter.4
